TPU v7x, 32 devices: a whole 2x2x4 slice. The times are simulated.
32 devices in a mesh: sp: 8 (over z, y), tp: 4 (over x, core).
Axes of the slice: x: 2, y: 2, z: 4, core: 2. Of those that a mesh axis runs over, the one named last changes fastest.
Arguments:
- queries: bfloat16 [8192, 1024], P('sp', 'tp'), may hold values from -300 to 300
- keys: bfloat16 [8192, 512], P('sp', 'tp'), may hold values from -6 to 6
- values: bfloat16 [8192, 512], P('sp', 'tp'), may hold values from -6 to 6
- sink_logits: float32 [16], P('tp'), may hold values from 1 to 6
- residual: bfloat16 [8192, 2048], P('sp'), may hold values from -3 to 3
- out_weight: bfloat16 [1024, 2048], P('tp'), may hold values from -0.5390625 to 0.5390625
- norm_gain: float32 [2048], replicated, may hold values from 0.1 to 1.9
- gate_weight: bfloat16 [2048, 5632], P('sp', 'tp'), may hold values from -0.125 to 0.125
- up_weight: bfloat16 [2048, 5632], P('sp', 'tp'), may hold values from -0.125 to 0.125
- down_weight: bfloat16 [2048, 5632], P('sp', 'tp'), may hold values from -0.1796875 to 0.1796875
Outputs:
- layer_out: bfloat16 [8192, 2048], P(('sp', 'tp'))
All inputs are finite; a program needn't handle non-finite values.
Results may differ from a plain program's by a relative error of at most 0.02.
Values may be sent and summed in bfloat16 or wider, within the bound.
No kernel may reach another device: no remote copies, remote signals or barrier semaphores. Data moves between devices by JAX's collectives and lax.ppermute only.
A program may use at most 64 MiB of HBM per device.

v0:
```python
import jax
import jax.numpy as jnp
from jax import lax
from jax.sharding import PartitionSpec as P

QH = 16
HD = 64
WINDOW = 128


def shifted(block, axis, distance):
    devices = range(lax.axis_size(axis))
    route = [(i - distance, i) for i in devices if i - distance in devices]
    return lax.ppermute(block, axis, route)


def attend(queries, keys, values, sink_logits):
    local_rows = queries.shape[0]
    kv_local = keys.shape[1] // HD
    heads_local = queries.shape[1] // HD
    groups = heads_local // kv_local
    blocks = local_rows // WINDOW
    key_value = jnp.concatenate([keys, values], axis=1)
    previous = shifted(key_value[local_rows - WINDOW :], "sp", 1)
    extended = jnp.concatenate([previous, key_value], axis=0)
    stacked = extended.reshape(blocks + 1, WINDOW, 2 * kv_local * HD)
    band = jnp.concatenate([stacked[:-1], stacked[1:]], axis=1)
    key_band = band[:, :, : kv_local * HD].reshape(blocks, 2 * WINDOW, kv_local, HD)
    value_band = band[:, :, kv_local * HD :].reshape(blocks, 2 * WINDOW, kv_local, HD)
    query_blocks = queries.reshape(blocks, WINDOW, kv_local, groups, HD)
    query_index = jnp.arange(WINDOW, dtype=jnp.int32)[:, None]
    key_index = jnp.arange(2 * WINDOW, dtype=jnp.int32)[None, :]
    distance = query_index - key_index + WINDOW
    offset = lax.axis_index("sp") * local_rows
    key_place = (
        offset
        + jnp.arange(blocks, dtype=jnp.int32)[:, None, None] * WINDOW
        + key_index[None]
        - WINDOW
    )
    valid = (distance >= 0) & (distance < WINDOW) & (key_place >= 0)
    head_number = (
        lax.axis_index("tp") * heads_local + jnp.arange(heads_local, dtype=jnp.int32) + 1
    ).astype(jnp.float32)
    slopes = (2.0 ** (-8.0 * head_number / QH)).reshape(kv_local, groups, 1, 1, 1)
    scores = jnp.einsum(
        "nqhgd,nkhd->hgnqk", query_blocks, key_band, preferred_element_type=jnp.float32
    ) * HD ** (-0.5)
    scores = scores - slopes * distance.astype(jnp.float32)
    scores = jnp.where(valid, scores, -jnp.inf)
    sinks = sink_logits.reshape(kv_local, groups, 1, 1, 1)
    top = jnp.maximum(jnp.max(scores, axis=-1, keepdims=True), sinks)
    expd = jnp.exp(scores - top)
    denom = jnp.sum(expd, axis=-1, keepdims=True) + jnp.exp(sinks - top)
    weights = (expd / denom).astype(jnp.bfloat16)
    output = jnp.einsum(
        "hgnqk,nkhd->nqhgd", weights, value_band, preferred_element_type=jnp.float32
    )
    return output.reshape(local_rows, heads_local * HD).astype(jnp.bfloat16)


def rms_scale(rows, norm_gain):
    rows_f = rows.astype(jnp.float32)
    scale = lax.rsqrt(jnp.mean(rows_f * rows_f, axis=-1, keepdims=True) + 1e-06)
    return (rows_f * scale * norm_gain).astype(jnp.bfloat16)


def expand_rows(normed, gate_full, up_full):
    gate = jnp.dot(normed, gate_full, preferred_element_type=jnp.float32)
    upper = jnp.dot(normed, up_full, preferred_element_type=jnp.float32)
    return (jax.nn.silu(gate) * upper).astype(jnp.bfloat16)


def per_device(
    queries,
    keys,
    values,
    sink_logits,
    residual,
    out_weight,
    norm_gain,
    gate_weight,
    up_weight,
    down_weight,
):
    attended = attend(queries, keys, values, sink_logits)
    local_rows = queries.shape[0]
    tp_count = lax.axis_size("tp")
    own_rows = local_rows // tp_count
    first_row = lax.axis_index("tp") * own_rows
    partial_sum = jnp.dot(attended, out_weight, preferred_element_type=jnp.float32)
    projected = lax.psum(partial_sum.astype(jnp.bfloat16), "tp").astype(jnp.float32)
    mixed_all = (residual.astype(jnp.float32) + projected).astype(jnp.bfloat16)
    mixed_rows = lax.dynamic_slice_in_dim(mixed_all, first_row, own_rows, 0)
    gate_full, up_full = (
        lax.all_gather(gate_weight, "sp", axis=0, tiled=True),
        lax.all_gather(up_weight, "sp", axis=0, tiled=True),
    )
    hidden = expand_rows(rms_scale(mixed_all, norm_gain), gate_full, up_full)
    down_full = lax.all_gather(down_weight, "sp", axis=0, tiled=True)
    expanded = lax.psum_scatter(
        lax.dot_general(
            hidden, down_full, (((1,), (1,)), ((), ())), preferred_element_type=jnp.float32
        ).astype(jnp.bfloat16),
        "tp",
        scatter_dimension=0,
        tiled=True,
    ).astype(jnp.float32)
    return (mixed_rows.astype(jnp.float32) + 0.5 * expanded).astype(jnp.bfloat16)


def solution(mesh):
    return jax.shard_map(
        per_device,
        mesh=mesh,
        in_specs=(
            P("sp", "tp"),
            P("sp", "tp"),
            P("sp", "tp"),
            P("tp"),
            P("sp", None),
            P("tp", None),
            P(),
            P("sp", "tp"),
            P("sp", "tp"),
            P("sp", "tp"),
        ),
        out_specs=P(("sp", "tp"), None),
        check_vma=False,
    )
```

profile of v0, /device:TPU:0, one launch (start us, length us, event | category | flops | bytes accessed | tf_op | source)
XLA Modules:
  0.0 386.4 jit_solution(11114447815396450490)
XLA Ops:
  7.4 1.1 constant_dynamic-update-slice_fusion.1
  8.5 1.0 constant_dynamic-update-slice_fusion
  9.5 4.9 %collective-permute-start = (bf16[128,256]{1,0:T(8,128)(2,1)S(1)}, bf16[128,256]{1,0:T(8,128)(2,1)S(1)}, u32[]{:S(2)}, u32[]{:S(2)}) collective-permute-start(bf16[128,256]{1,0:T(8,128)(2,1)S(1)} %slice.25), channel_id=1, source_target_pairs={{0,4},{4,8},{8,12},{12,16},{16,20},{20,24},{24,28},{1,5},{5,9},{9,... | collective-permute-start | bytes 196616 | tf_op jit(solution)/shard_map/ppermute | solution.py:14
  14.7 0.3 broadcast_and_fusion
  15.0 3.2 reshape.128
  18.3 0.7 max.18
  19.5 2.3 fusion.5
  22.0 1.9 copy-done.1
  23.8 1.1 fusion.4
  25.3 3.5 fusion.11
  28.7 0.3 copy.26
  29.1 3.3 convolution_convert_fusion.1
  32.5 0.5 all-gather.4.cloned.1.call-update
  33.0 0.5 all-gather.6.cloned.1.call-update
  33.6 0.5 all-gather.8.cloned.1.call-update
  34.4 83.9 %all-reduce.2.cloned.1.call-done = bf16[1024,2048]{1,0:T(8,128)(2,1)} async-done(((bf16[1024,2048]{1,0:T(8,128)(2,1)}), bf16[1024,2048]{1,0:T(8,128)(2,1)}) %all-reduce.2.cloned.1.call-update) | async-done | bytes 4194320 | tf_op jit(solution)/shard_map/psum | solution.py:92
  118.4 7.5 %fusion = (f32[1024]{0:T(1024)S(1)}, bf16[1024,2048]{1,0:T(8,128)(2,1)}) fusion(bf16[1024,2048]{1,0:T(8,128)(2,1)} %all-reduce.2.cloned.1.call-done, bf16[1024,2048]{1,0:T(8,128)(2,1)} %param.14), kind=kLoop, calls=%fused_computation.2 | loop fusion | flops 14679040 | bytes 12587008 | tf_op jit(solution)/shard_map/reduce_sum | solution.py:64
  125.8 1.7 all-gather.4.cloned.1.call-done
  127.5 11.9 %fusion.15 = f32[1024,1408]{1,0:T(8,128)} fusion(bf16[2048,1408]{1,0:T(8,128)(2,1)} %all-gather.4.cloned.1.call-done, bf16[1024,2048]{1,0:T(8,128)(2,1)} %get-tuple-element.6, f32[2048]{0:T(1024)S(1)} %copy-done.2, f32[1024]{0:T(1024)S(1)} %add_rsqrt_fusion), kind=kOutput, calls=%fused_computation.20 | convolution fusion | flops 5913968640 | bytes 15740928 | tf_op jit(solution)/shard_map/dot_general | solution.py:69
  139.5 80.4 %all-gather.6.cloned.1.call-done = bf16[2048,1408]{1,0:T(8,128)(2,1)} async-done(((bf16[256,1408]{1,0:T(8,128)(2,1)}), bf16[2048,1408]{1,0:T(8,128)(2,1)}) %all-gather.6.cloned.1.call-update) | async-done | bytes 5767184 | tf_op jit(solution)/shard_map/all_gather | solution.py:97
  219.9 92.4 %all-gather.8.cloned.1.call-done = bf16[2048,1408]{1,0:T(8,128)(2,1)} async-done(((bf16[256,1408]{1,0:T(8,128)(2,1)}), bf16[2048,1408]{1,0:T(8,128)(2,1)}) %all-gather.8.cloned.1.call-update) | async-done | bytes 5767184 | tf_op jit(solution)/shard_map/all_gather | solution.py:100
  312.2 20.8 %convolution_convert_fusion = bf16[1024,2048]{1,0:T(8,128)(2,1)} fusion(bf16[2048,1408]{1,0:T(8,128)(2,1)} %all-gather.8.cloned.1.call-done, f32[1024,1408]{1,0:T(8,128)} %fusion.15, bf16[2048,1408]{1,0:T(8,128)(2,1)} %all-gather.6.cloned.1.call-done, bf16[1024,2048]{1,0:T(8,128)(2,1)} %get-tuple-element.6, f32[2048]{0:T(1024)S(1)} %copy-done.2, ...), kind=kOutput, calls=%fused_computation.11 | convolution fusion | flops 11830296576 | bytes 25702400 | tf_op jit(solution)/shard_map/dot_general | solution.py:102
  333.1 42.8 %reduce-scatter.2.cloned.1.call-done = bf16[256,2048]{1,0:T(8,128)(2,1)} async-done(((bf16[1024,2048]{1,0:T(8,128)(2,1)}), bf16[256,2048]{1,0:T(8,128)(2,1)}) %reduce-scatter.2.cloned.1.call-update) | async-done | bytes 1048592 | tf_op jit(solution)/shard_map/reduce_scatter | solution.py:101
  375.9 2.9 add_convert_fusion.1
  (27 shorter events, 1.6 us)
Async XLA Ops:
  7.4 21.7 %copy-start = (bf16[256,2048]{1,0:T(8,128)(2,1)S(1)}, bf16[256,2048]{1,0:T(8,128)(2,1)}, u32[]{:S(2)}) copy-start(bf16[256,2048]{1,0:T(8,128)(2,1)} %param.15) | copy-start | bytes 3145732
  7.4 111.0 %all-reduce.2.cloned.1.call-start = ((), (), s32[]{:S(2)}) async-start(), calls=%async_computation.1 | async-start | bytes 8388608 | tf_op jit(solution)/shard_map/psum | solution.py:92
  9.5 9.5 %collective-permute-start = (bf16[128,256]{1,0:T(8,128)(2,1)S(1)}, bf16[128,256]{1,0:T(8,128)(2,1)S(1)}, u32[]{:S(2)}, u32[]{:S(2)}) collective-permute-start(bf16[128,256]{1,0:T(8,128)(2,1)S(1)} %slice.25), channel_id=1, source_target_pairs={{0,4},{4,8},{8,12},{12,16},{16,20},{20,24},{24,28},{1,5},{5,9},{9,... | collective-permute-start | bytes 196616 | tf_op jit(solution)/shard_map/ppermute | solution.py:14
  21.9 1.9 copy-start.1
  32.4 95.1 %all-gather.4.cloned.1.call-start = ((), (), s32[]{:S(2)}) async-start(), calls=%async_computation.2 | async-start | bytes 6488064 | tf_op jit(solution)/shard_map/all_gather | solution.py:96
  33.0 186.9 %all-gather.6.cloned.1.call-start = ((), (), s32[]{:S(2)}) async-start(), calls=%async_computation.3 | async-start | bytes 6488064 | tf_op jit(solution)/shard_map/all_gather | solution.py:97
  33.6 278.7 %all-gather.8.cloned.1.call-start = ((), (), s32[]{:S(2)}) async-start(), calls=%async_computation.4 | async-start | bytes 6488064 | tf_op jit(solution)/shard_map/all_gather | solution.py:100
  34.2 93.4 %copy-start.2 = (f32[2048]{0:T(1024)S(1)}, f32[2048]{0:T(1024)}, u32[]{:S(2)}) copy-start(f32[2048]{0:T(1024)} %param.16) | copy-start | bytes 24580
  34.2 341.8 %reduce-scatter.2.cloned.1.call-start = ((), (), s32[]{:S(2)}) async-start(), calls=%async_computation.5 | async-start | bytes 5242880 | tf_op jit(solution)/shard_map/reduce_scatter | solution.py:101
Sparse Core Ops, SparseCore 0:
  32.5 85.7 all-reduce.1
  333.2 42.6 reduce-scatter.1
Sparse Core Ops, SparseCore 1:
  35.1 92.4 all-gather.3
  129.6 90.2 all-gather.5
  222.0 90.2 all-gather.7
where the time goes:
time: 387 us; the launch traced here: 386 us
  waiting for transfers between devices  303 us (78%)
  matrix products  41.9 us (11%)
  between operations  15.2 us (4%)
  other arithmetic  12.5 us (3%)
  local copies, waits for them, and re-layouts  8.71 us (2%)
  starting transfers between devices  5.25 us (1%)
    all_gather x1, waiting for transfers between devices, per_device(): down_full = lax.all_gather(down_weight, 'sp', axis=0, tiled=True)  92.4 us
    psum x1, waiting for transfers between devices, per_device(): lax.psum(partial_sum.astype(jnp.bfloat16), 'tp').astype(jnp.float32)  83.9 us
    all_gather x1, waiting for transfers between devices, per_device(): lax.all_gather(up_weight, 'sp', axis=0, tiled=True)  80.4 us
    reduce_scatter x1, waiting for transfers between devices, per_device(): lax.psum_scatter(lax.dot_general(hidden, down_full, (((1,), (1,)), ((), (...  42.8 us
    dot_general x1, matrix products, per_device(): lax.dot_general(hidden, down_full, (((1,), (1,)), ((), ())), preferred_el...  20.8 us
    dot_general x1, matrix products, expand_rows(): gate = jnp.dot(normed, gate_full, preferred_element_type=jnp.float32)  11.9 us
  transfers between devices with their start and end apart: 6, of which 5 were waited for; matrix products, arithmetic and copies ran while one was open for 6% of the time, Pallas kernels for 0%

commit v1 on v0

--- a/solution.py
+++ b/solution.py
@@ -89,7 +89,9 @@
     own_rows = local_rows // tp_count
     first_row = lax.axis_index("tp") * own_rows
     partial_sum = jnp.dot(attended, out_weight, preferred_element_type=jnp.float32)
-    projected = lax.psum(partial_sum.astype(jnp.bfloat16), "tp").astype(jnp.float32)
+    projected = jnp.sum(lax.all_gather(partial_sum.astype(jnp.bfloat16), "tp"), axis=0).astype(
+        jnp.float32
+    )
     mixed_all = (residual.astype(jnp.float32) + projected).astype(jnp.bfloat16)
     mixed_rows = lax.dynamic_slice_in_dim(mixed_all, first_row, own_rows, 0)
     gate_full, up_full = (

time: 387 us -> 491 us (1.27)
  waiting for transfers between devices: 303 us -> 397 us
  other arithmetic: 12.5 us -> 24.7 us
    all_gather x0 -> x1, waiting for transfers between devices: none -> 104 us  [per_device(): lax.all_gather(partial_sum.astype(jnp.bfloat16), 'tp')]
    psum x1 -> x0, waiting for transfers between devices: 83.9 us -> none  [per_device(): lax.psum(partial_sum.astype(jnp.bfloat16), 'tp').astype(jnp.float32)]
    all_gather x1, waiting for transfers between devices: 1.72 us -> 74.9 us  [per_device(): lax.all_gather(gate_weight, 'sp', axis=0, tiled=True)]
    all_gather x1, waiting for transfers between devices: 80.4 us -> 92.6 us  [per_device(): lax.all_gather(up_weight, 'sp', axis=0, tiled=True)]
    reduce_sum x0 -> x1, other arithmetic: none -> 12.1 us  [per_device(): jnp.sum(lax.all_gather(partial_sum.astype(jnp.bfloat16), 'tp'), axis=0)]
    all_gather x1, waiting for transfers between devices: 92.4 us -> 80.8 us  [per_device(): down_full = lax.all_gather(down_weight, 'sp', axis=0, tiled=True)]
  transfers between devices with their start and end apart: 6 -> 6, of which waited for: 5 -> 5; matrix products, arithmetic and copies ran while one was open for 6% -> 7% of each run, Pallas kernels for 0% -> 0%
where the time goes in v1:
time: 491 us
  waiting for transfers between devices  397 us (81%)
  matrix products  42 us (9%)
  other arithmetic  24.7 us (5%)
  between operations  13.3 us (3%)
  local copies, waits for them, and re-layouts  8.71 us (2%)
  starting transfers between devices  5.24 us (1%)
    all_gather x1, waiting for transfers between devices, per_device(): lax.all_gather(partial_sum.astype(jnp.bfloat16), 'tp')  104 us
    all_gather x1, waiting for transfers between devices, per_device(): lax.all_gather(up_weight, 'sp', axis=0, tiled=True)  92.6 us
    all_gather x1, waiting for transfers between devices, per_device(): down_full = lax.all_gather(down_weight, 'sp', axis=0, tiled=True)  80.8 us
    all_gather x1, waiting for transfers between devices, per_device(): lax.all_gather(gate_weight, 'sp', axis=0, tiled=True)  74.9 us
    reduce_scatter x1, waiting for transfers between devices, per_device(): lax.psum_scatter(lax.dot_general(hidden, down_full, (((1,), (1,)), ((), (...  42.9 us
    dot_general x1, matrix products, per_device(): lax.dot_general(hidden, down_full, (((1,), (1,)), ((), ())), preferred_el...  21 us
    reduce_sum x1, other arithmetic, per_device(): jnp.sum(lax.all_gather(partial_sum.astype(jnp.bfloat16), 'tp'), axis=0)  12.1 us
    dot_general x1, matrix products, expand_rows(): gate = jnp.dot(normed, gate_full, preferred_element_type=jnp.float32)  11.9 us
  transfers between devices with their start and end apart: 6, of which 5 were waited for; matrix products, arithmetic and copies ran while one was open for 7% of the time, Pallas kernels for 0%

profile of v1, /device:TPU:0, one launch (start us, length us, event | category | flops | bytes accessed | tf_op | source)
XLA Modules:
  0.0 491.1 jit_solution(1010937267561818469)
XLA Ops:
  6.5 1.1 constant_dynamic-update-slice_fusion.1
  7.6 1.0 constant_dynamic-update-slice_fusion
  8.7 4.9 collective-permute-start
  14.2 3.2 reshape.129
  17.4 0.7 max.18
  18.7 2.3 fusion.5
  21.1 1.9 copy-done.2
  23.0 1.1 fusion.4
  24.4 3.5 fusion.11
  27.9 0.3 copy.26
  28.2 3.3 convolution_convert_fusion.1
  31.6 0.7 all-gather.6.cloned.1.call-update
  32.4 0.7 all-gather.10.cloned.1.call-update
  33.1 0.5 all-gather.8.cloned.1.call-update
  33.9 104.1 %all-gather.12.cloned.1.call-done = bf16[4096,2048]{1,0:T(8,128)(2,1)} async-done(((bf16[1024,2048]{1,0:T(8,128)(2,1)}), bf16[4096,2048]{1,0:T(8,128)(2,1)}) %all-gather.12.cloned.1.call-update) | async-done | bytes 16777232 | tf_op jit(solution)/shard_map/all_gather | solution.py:92
  137.9 12.1 %reduce_sum.31 = bf16[1024,2048]{1,0:T(8,128)(2,1)} reduce(bf16[4,1024,2048]{2,1,0:T(8,128)(2,1)} %bitcast.42, bf16[]{:T(256)} %constant.48.clone.1), dimensions={0}, to_apply=%region_2.3 | reduce | flops 6291456 | bytes 20971522 | tf_op jit(solution)/shard_map/reduce_sum | solution.py:92
  150.1 7.5 %fusion = (f32[1024]{0:T(1024)S(1)}, bf16[1024,2048]{1,0:T(8,128)(2,1)}) fusion(bf16[1024,2048]{1,0:T(8,128)(2,1)} %reduce_sum.31, bf16[1024,2048]{1,0:T(8,128)(2,1)} %param.14), kind=kLoop, calls=%fused_computation.2 | loop fusion | flops 14679040 | bytes 12587008 | tf_op jit(solution)/shard_map/reduce_sum | solution.py:64
  157.6 74.9 %all-gather.6.cloned.1.call-done = bf16[2048,1408]{1,0:T(8,128)(2,1)} async-done(((bf16[256,1408]{1,0:T(8,128)(2,1)}), bf16[2048,1408]{1,0:T(8,128)(2,1)}) %all-gather.6.cloned.1.call-update) | async-done | bytes 5767184 | tf_op jit(solution)/shard_map/all_gather | solution.py:98
  232.5 11.9 %fusion.15 = f32[1024,1408]{1,0:T(8,128)} fusion(bf16[2048,1408]{1,0:T(8,128)(2,1)} %all-gather.6.cloned.1.call-done, bf16[1024,2048]{1,0:T(8,128)(2,1)} %get-tuple-element.6, f32[2048]{0:T(1024)S(1)} %copy-done.3, f32[1024]{0:T(1024)S(1)} %add_rsqrt_fusion), kind=kOutput, calls=%fused_computation.20 | convolution fusion | flops 5913968640 | bytes 15740928 | tf_op jit(solution)/shard_map/dot_general | solution.py:69
  244.4 80.8 %all-gather.10.cloned.1.call-done = bf16[2048,1408]{1,0:T(8,128)(2,1)} async-done(((bf16[256,1408]{1,0:T(8,128)(2,1)}), bf16[2048,1408]{1,0:T(8,128)(2,1)}) %all-gather.10.cloned.1.call-update) | async-done | bytes 5767184 | tf_op jit(solution)/shard_map/all_gather | solution.py:102
  325.2 92.6 %all-gather.8.cloned.1.call-done = bf16[2048,1408]{1,0:T(8,128)(2,1)} async-done(((bf16[256,1408]{1,0:T(8,128)(2,1)}), bf16[2048,1408]{1,0:T(8,128)(2,1)}) %all-gather.8.cloned.1.call-update) | async-done | bytes 5767184 | tf_op jit(solution)/shard_map/all_gather | solution.py:99
  417.7 21.0 %convolution_convert_fusion = bf16[1024,2048]{1,0:T(8,128)(2,1)} fusion(bf16[2048,1408]{1,0:T(8,128)(2,1)} %all-gather.10.cloned.1.call-done, f32[1024,1408]{1,0:T(8,128)} %fusion.15, bf16[2048,1408]{1,0:T(8,128)(2,1)} %all-gather.8.cloned.1.call-done, bf16[1024,2048]{1,0:T(8,128)(2,1)} %get-tuple-element.6, f32[2048]{0:T(1024)S(1)} %copy-done.3, ...), kind=kOutput, calls=%fused_computation.11 | convolution fusion | flops 11830296576 | bytes 25702400 | tf_op jit(solution)/shard_map/dot_general | solution.py:104
  438.7 42.9 %reduce-scatter.2.cloned.1.call-done = bf16[256,2048]{1,0:T(8,128)(2,1)} async-done(((bf16[1024,2048]{1,0:T(8,128)(2,1)}), bf16[256,2048]{1,0:T(8,128)(2,1)}) %reduce-scatter.2.cloned.1.call-update) | async-done | bytes 1048592 | tf_op jit(solution)/shard_map/reduce_scatter | solution.py:103
  481.6 2.9 add_convert_fusion.1
  (30 shorter events, 1.9 us)
Async XLA Ops:
  6.5 21.7 %copy-start = (bf16[256,2048]{1,0:T(8,128)(2,1)S(1)}, bf16[256,2048]{1,0:T(8,128)(2,1)}, u32[]{:S(2)}) copy-start(bf16[256,2048]{1,0:T(8,128)(2,1)} %param.15) | copy-start | bytes 3145732
  6.5 131.4 %all-gather.12.cloned.1.call-start = ((), (), s32[]{:S(2)}) async-start(), calls=%async_computation.5 | async-start | bytes 20971520 | tf_op jit(solution)/shard_map/all_gather | solution.py:92
  8.7 9.5 %collective-permute-start = (bf16[128,256]{1,0:T(8,128)(2,1)S(1)}, bf16[128,256]{1,0:T(8,128)(2,1)S(1)}, u32[]{:S(2)}, u32[]{:S(2)}) collective-permute-start(bf16[128,256]{1,0:T(8,128)(2,1)S(1)} %slice.25), channel_id=1, source_target_pairs={{0,4},{4,8},{8,12},{12,16},{16,20},{20,24},{24,28},{1,5},{5,9},{9,... | collective-permute-start | bytes 196616 | tf_op jit(solution)/shard_map/ppermute | solution.py:14
  21.1 1.9 copy-start.2
  31.6 200.9 %all-gather.6.cloned.1.call-start = ((), (), s32[]{:S(2)}) async-start(), calls=%async_computation.1 | async-start | bytes 6488064 | tf_op jit(solution)/shard_map/all_gather | solution.py:98
  32.3 292.8 %all-gather.10.cloned.1.call-start = ((), (), s32[]{:S(2)}) async-start(), calls=%async_computation.3 | async-start | bytes 6488064 | tf_op jit(solution)/shard_map/all_gather | solution.py:102
  33.1 384.7 %all-gather.8.cloned.1.call-start = ((), (), s32[]{:S(2)}) async-start(), calls=%async_computation.2 | async-start | bytes 6488064 | tf_op jit(solution)/shard_map/all_gather | solution.py:99
  33.7 448.0 %reduce-scatter.2.cloned.1.call-start = ((), (), s32[]{:S(2)}) async-start(), calls=%async_computation.4 | async-start | bytes 5242880 | tf_op jit(solution)/shard_map/reduce_scatter | solution.py:103
  150.1 82.4 %copy-start.3 = (f32[2048]{0:T(1024)S(1)}, f32[2048]{0:T(1024)}, u32[]{:S(2)}) copy-start(f32[2048]{0:T(1024)} %param.16) | copy-start | bytes 24580
  417.7 66.8 %copy-start.1 = (bf16[256,2048]{1,0:T(8,128)(2,1)S(1)}, bf16[256,2048]{1,0:T(8,128)(2,1)}, u32[]{:S(2)}) copy-start(bf16[256,2048]{1,0:T(8,128)(2,1)} %param.15) | copy-start | bytes 3145732
Sparse Core Ops, SparseCore 0:
  31.7 106.1 all-gather.11
  140.1 92.3 all-gather.5
  234.7 90.4 all-gather.9
  327.2 90.4 all-gather.7
  438.9 42.7 reduce-scatter.1
